TPU v7x, 256 devices: a whole 4x4x8 slice. The times are simulated.
256 devices in a mesh: ep: 32 (over z, x), tp: 8 (over y, core).
Axes of the slice: x: 4, y: 4, z: 8, core: 2. Of those that a mesh axis runs over, the one named last changes fastest.
Arguments:
- stream: bfloat16 [8192, 3072], P('ep'), may hold values from -30 to 30
- ffn_gain: bfloat16 [3072], replicated, may hold values from 0.099609375 to 1.8984375
- chosen: int32 [32, 1024], replicated, may hold values from 0 to 8191, as said below
- affinity: float32 [32, 1024], P('ep'), may hold values from 0.5 to 2
- w_gate: bfloat16 [32, 3072, 3072], P('ep', None, 'tp'), may hold values from -0.109375 to 0.109375
- w_up: bfloat16 [32, 3072, 3072], P('ep', None, 'tp'), may hold values from -0.109375 to 0.109375
- w_down: bfloat16 [32, 3072, 3072], P('ep', 'tp'), may hold values from -0.109375 to 0.109375
- final_gain: bfloat16 [3072], P('tp'), may hold values from 0.099609375 to 1.8984375
Outputs:
- normed: bfloat16 [8192, 3072], P('ep', 'tp')
Inputs may be any that keep to these rules, and one draw needn't show every extreme that they name: `chosen`: row e holds 1024 distinct token numbers in ascending order. Of the 256 tokens of one index of ep, each expert reads at least one and at most 48; in every draw some expert reads exactly 48 from some index.
All inputs are finite; a program needn't handle non-finite values.
Results may differ from a plain program's by a relative error of at most 0.015.
Values may be sent and summed in bfloat16 or wider, within the bound.
A program may use at most 128 MiB of HBM per device.

v0:
```python
import jax
import jax.numpy as jnp
from jax import lax
from jax.sharding import PartitionSpec as P

EPSILON = 1e-06


def sent_to_all(array, axis):
    devices = lax.axis_size(axis)
    return lax.all_to_all(
        jnp.broadcast_to(array[None], (devices, *array.shape)), axis, 0, 0, tiled=True
    )


def over_copies(array, axis):
    return sent_to_all(array, axis).sum(axis=0)


def on_device(stream, ffn_gain, chosen, affinity, w_gate, w_up, w_down, final_gain):
    tok_rows = stream.shape[0]
    model_width = stream.shape[1]
    experts = chosen.shape[0]
    picks = chosen.shape[1]
    ep_count = lax.axis_size("ep")
    tp_count = lax.axis_size("tp")
    device = lax.axis_index("ep")
    column = lax.axis_index("tp")
    share_width = model_width // tp_count
    slots = 3 * tok_rows // 16
    widened = stream.astype(jnp.float32)
    scale_in = lax.rsqrt(jnp.mean(widened * widened, axis=-1, keepdims=True) + EPSILON)
    normed_in = (widened * scale_in * ffn_gain.astype(jnp.float32)).astype(jnp.bfloat16)
    source = chosen // tok_rows
    counts = jnp.sum(
        (source[:, :, None] == jnp.arange(ep_count)[None, None, :]).astype(jnp.int32), axis=1
    )
    starts = jnp.cumsum(counts, axis=1) - counts
    slot_range = jnp.arange(slots, dtype=jnp.int32)
    own_start = jnp.take(starts, device, axis=1)
    own_count = jnp.take(counts, device, axis=1)
    send_pos = jnp.clip(own_start[:, None] + slot_range[None, :], 0, picks - 1)
    send_valid = slot_range[None, :] < own_count[:, None]
    local_tok = jnp.where(
        send_valid, jnp.take_along_axis(chosen, send_pos, axis=1) - device * tok_rows, 0
    )
    local_flat = local_tok.reshape(-1)
    row_source = jnp.take(source, device, axis=0)
    row_starts = jnp.take(starts, device, axis=0)
    arrival = (
        row_source * slots + jnp.arange(picks, dtype=jnp.int32) - jnp.take(row_starts, row_source)
    )
    gate_rows = w_gate[0]
    up_rows = w_up[0]
    own_columns = lax.dynamic_slice_in_dim(normed_in, column * share_width, share_width, 1)
    outgoing = jnp.take(own_columns, local_flat, axis=0).reshape(experts, slots, share_width)
    arrived = lax.all_to_all(outgoing, "ep", split_axis=0, concat_axis=0, tiled=True)
    shared = jnp.take(arrived.reshape(-1, share_width), arrival, axis=0)
    piece = lax.all_gather(shared, "tp", axis=1, tiled=True)
    gate = jnp.dot(piece, gate_rows, preferred_element_type=jnp.float32)
    up = jnp.dot(piece, up_rows, preferred_element_type=jnp.float32)
    hidden = (jax.nn.silu(gate) * up).astype(jnp.bfloat16)
    down_rows = w_down[0]
    piece = down_rows
    expert_cols = lax.psum_scatter(
        lax.dot_general(
            piece, hidden, (((0,), (1,)), ((), ())), preferred_element_type=jnp.float32
        ).astype(jnp.bfloat16),
        "tp",
        scatter_dimension=0,
        tiled=True,
    ).astype(jnp.float32)
    weighted = (expert_cols * affinity[0][None, :]).astype(jnp.bfloat16)
    slot_pos = jnp.clip(row_starts[:, None] + slot_range[None, :], 0, picks - 1)
    leaving = jnp.take(weighted, slot_pos.reshape(-1), axis=1).reshape(share_width, ep_count, slots)
    returned = lax.all_to_all(leaving, "ep", split_axis=1, concat_axis=1, tiled=True)
    placing = (
        (local_flat[:, None] == jnp.arange(tok_rows, dtype=jnp.int32)[None, :])
        & send_valid.reshape(-1)[:, None]
    ).astype(jnp.bfloat16)
    update = lax.dot_general(
        placing,
        returned.reshape(share_width, -1),
        (((0,), (1,)), ((), ())),
        preferred_element_type=jnp.float32,
    )
    own_stream = lax.dynamic_slice_in_dim(widened, column * share_width, share_width, 1)
    merged = own_stream + update
    totals = over_copies(jnp.sum(merged * merged, axis=1), "tp")
    scale_out = lax.rsqrt(totals[:, None] / model_width + EPSILON)
    return (merged * scale_out * final_gain.astype(jnp.float32)[None, :]).astype(jnp.bfloat16)


def solution(mesh):
    return jax.shard_map(
        on_device,
        mesh=mesh,
        in_specs=(
            P("ep", None),
            P(),
            P(),
            P("ep", None),
            P("ep", None, "tp"),
            P("ep", None, "tp"),
            P("ep", "tp", None),
            P("tp"),
        ),
        out_specs=P("ep", "tp"),
        check_vma=False,
    )
```

profile of v0, /device:TPU:1, one launch (start us, length us, event | category | flops | bytes accessed | tf_op | source)
XLA Modules:
  0.0 273.2 jit_solution(4535225694800903247)
XLA Ops:
  6.5 2.0 multiply_reduce_fusion
  8.5 0.1 copy-done.2
  8.6 2.0 convert_element_type.34
  10.6 0.1 lt.201
  10.7 0.1 add_select_fusion
  10.8 0.0 copy-start.3
  10.8 0.6 copy-done.3
  11.5 0.6 convert_reduce_fusion
  12.1 0.2 reduce_window_sum.11
  12.3 0.2 select_reduce_fusion
  12.5 0.1 fusion.21
  12.6 0.1 add.254
  12.7 0.6 copy-done.4
  13.3 0.1 add.280
  13.3 0.1 reshape.527
  13.4 12.6 %gather_fusion.3 = s32[1536]{0:T(1024)S(1)} fusion(s32[32,1024]{1,0:T(8,128)S(1)} %copy-done.1, s32[1536]{0:T(1024)S(1)} %reshape.527), kind=kCustom, calls=%fused_computation.3 | custom fusion | bytes 24576 | tf_op jit(solution)/shard_map/jit(take_along_axis)/gather | solution.py:45
  26.0 0.1 reshape.530
  26.1 0.1 compare_and_fusion
  26.2 0.1 lt.199
  26.3 0.1 fusion.25
  26.4 0.8 dynamic-slice.15
  27.2 1.1 multiply_convert_fusion.3
  28.3 5.3 %gather_fusion = bf16[1536,384]{1,0:T(8,128)(2,1)} fusion(bf16[256,384]{1,0:T(8,128)(2,1)S(1)} %multiply_convert_fusion.3, s32[2048]{0:T(1024)S(1)} %pad_clamp_fusion.1), kind=kCustom, calls=%fused_computation | custom fusion | bytes 2365440 | tf_op jit(solution)/shard_map/jit(_take)/gather | solution.py:56
  33.6 2.6 broadcast_select_fusion
  36.1 11.9 %all-to-all-start = ((bf16[32,48,384]{2,1,0:T(8,128)(2,1)}), bf16[32,48,384]{2,1,0:T(8,128)(2,1)S(1)}, u32[]{:S(2)}, u32[]{:S(2)}) async-start(bf16[32,48,384]{2,1,0:T(8,128)(2,1)} %broadcast_select_fusion), calls=%async_computation | async-start | bytes 2359296 | tf_op jit(solution)/shard_map/all_to_all | solution.py:57
  48.0 0.0 all-gather.2.cloned.1.call-start
  48.0 0.7 broadcast_select_fusion.4
  48.7 0.7 fusion.30
  49.5 4.9 %compare_select_fusion.10 = (s32[1024,1]{0,1:T(1,128)S(1)}, s32[1024,1]{0,1:T(1,128)S(1)}, s32[1,1024]{1,0:T(1,128)S(1)}) fusion(s32[]{:T(128)} %bitcast.28, s32[]{:T(128)} %bitcast.29, s32[]{:T(128)} %bitcast.30, s32[]{:T(128)} %bitcast.31, s32[]{:T(128)} %bitcast.32, s32[]{:T(128)} %bitcast.34, s32[]{:T(128)} %bitcast.33, s32[32,1024]{1,0:T(8,128)} %copy-done.3, ...), kind=kLoop, calls=%fused_computation.80 | loop fusion | flops 16384 | bytes 16417 | tf_op jit(solution)/shard_map/jit(_take)/gather | solution.py:51
  54.4 0.7 fusion.31
  55.1 0.3 compare_reduce_fusion.24
  55.3 16.2 %compare_and_fusion.2 = (pred[1024]{0:T(1024)(128)(4,1)}, s32[1024]{0:T(1024)S(1)}) fusion(s32[1024]{0:T(1024)S(1)} %bitcast.88, pred[1024]{0:T(1024)(128)(4,1)S(1)} %get-tuple-element.63, pred[1024]{0:T(1024)(128)(4,1)S(1)} %get-tuple-element.61, pred[1024]{0:T(1024)(128)(4,1)S(1)} %get-tuple-element.62, pred[1024]{0:T(1024)(128)(4,1)S(1)} %get-tuple-element.60, ...), kind=kLoop, calls=%fused_computation.101 | loop fusion | flops 41984 | bytes 39012 | tf_op jit(solution)/shard_map/jit(_take)/and | solution.py:58
  71.6 5.1 %all-to-all-done = bf16[32,48,384]{2,1,0:T(8,128)(2,1)S(1)} async-done(((bf16[32,48,384]{2,1,0:T(8,128)(2,1)}), bf16[32,48,384]{2,1,0:T(8,128)(2,1)S(1)}, u32[]{:S(2)}, u32[]{:S(2)}) %all-to-all-start) | async-done | bytes 1179680 | tf_op jit(solution)/shard_map/all_to_all | solution.py:57
  76.7 5.0 %gather_fusion.1 = bf16[1024,384]{1,0:T(8,128)(2,1)} fusion(bf16[1536,384]{1,0:T(8,128)(2,1)S(1)} %bitcast.84, s32[1024]{0:T(1024)S(1)} %broadcast_clamp_fusion), kind=kCustom, calls=%fused_computation.1 | custom fusion | bytes 1576960 | tf_op jit(solution)/shard_map/jit(_take)/gather | solution.py:58
  81.6 2.2 broadcast_select_fusion.2
  83.9 0.0 all-gather.2.cloned.1.call-update
  83.9 0.0 reduce-scatter.4.cloned.1.call-start
  83.9 43.6 %all-gather.2.cloned.1.call-done = bf16[1024,3072]{1,0:T(8,128)(2,1)} async-done(((bf16[1024,384]{1,0:T(8,128)(2,1)}), bf16[1024,3072]{1,0:T(8,128)(2,1)}) %all-gather.2.cloned.1.call-update) | async-done | bytes 6291472 | tf_op jit(solution)/shard_map/all_gather | solution.py:59
  127.5 8.0 %fusion.3 = f32[1024,384]{1,0:T(8,128)} fusion(bf16[1024,3072]{1,0:T(8,128)(2,1)} %all-gather.2.cloned.1.call-done, bf16[1,3072,384]{2,1,0:T(8,128)(2,1)} %param.14), kind=kOutput, calls=%fused_computation.11 | convolution fusion | flops 2415919104 | bytes 10223616 | tf_op jit(solution)/shard_map/dot_general | solution.py:60
  135.5 11.4 %convert_bitcast_fusion = bf16[3072,1024]{0,1:T(8,128)(2,1)} fusion(bf16[1,384,3072]{2,1,0:T(8,128)(2,1)S(1)} %copy-done, f32[1024,384]{1,0:T(8,128)} %fusion.3, bf16[1024,3072]{1,0:T(8,128)(2,1)} %all-gather.2.cloned.1.call-done, bf16[1,3072,384]{2,1,0:T(8,128)(2,1)} %param.15), kind=kOutput, calls=%fused_computation.4 | convolution fusion | flops 4837343232 | bytes 18874368 | tf_op jit(solution)/shard_map/dot_general | solution.py:66
  146.9 8.7 %copy.10 = bf16[3072,1024]{1,0:T(8,128)(2,1)} copy(bf16[3072,1024]{0,1:T(8,128)(2,1)} %convert_bitcast_fusion) | data formatting | bytes 12582912
  155.6 0.0 reduce-scatter.4.cloned.1.call-update
  155.6 0.0 copy-start.6
  155.6 0.7 fusion.35
  156.3 0.1 add_clamp_fusion
  156.4 0.1 min.35
  156.5 0.1 compare_and_fusion.1
  156.6 43.4 %reduce-scatter.4.cloned.1.call-done = bf16[384,1024]{1,0:T(8,128)(2,1)} async-done(((bf16[3072,1024]{1,0:T(8,128)(2,1)}), bf16[384,1024]{1,0:T(8,128)(2,1)}) %reduce-scatter.4.cloned.1.call-update) | async-done | bytes 786448
  200.0 2.3 copy.11
  202.3 1.3 multiply_convert_fusion
  203.6 5.3 %gather_fusion.2 = bf16[1536,384]{1,0:T(8,128)(2,1)} fusion(bf16[384,1024]{0,1:T(8,128)(2,1)S(1)} %multiply_convert_fusion, s32[2048]{0:T(1024)S(1)} %pad_clamp_fusion), kind=kCustom, calls=%fused_computation.2 | custom fusion | bytes 2365440 | tf_op jit(solution)/shard_map/jit(_take)/gather | solution.py:75
  208.9 2.6 broadcast_select_fusion.1
  211.5 9.5 %all-to-all-start.1 = ((bf16[384,32,48]{0,2,1:T(8,128)(2,1)}), bf16[384,32,48]{0,2,1:T(8,128)(2,1)S(1)}, u32[]{:S(2)}, u32[]{:S(2)}) async-start(bf16[384,32,48]{0,2,1:T(8,128)(2,1)} %broadcast_select_fusion.1), calls=%async_computation.1 | async-start | bytes 2359296 | tf_op jit(solution)/shard_map/all_to_all | solution.py:76
  221.0 1.4 add.255
  222.4 0.7 lt.182
  223.1 0.6 lt.183
  223.7 0.8 lt.184
  224.5 1.3 subtract_select_fusion
  225.8 23.7 %all-to-all-done.1 = bf16[384,32,48]{0,2,1:T(8,128)(2,1)S(1)} async-done(((bf16[384,32,48]{0,2,1:T(8,128)(2,1)}), bf16[384,32,48]{0,2,1:T(8,128)(2,1)S(1)}, u32[]{:S(2)}, u32[]{:S(2)}) %all-to-all-start.1) | async-done | bytes 1179680 | tf_op jit(solution)/shard_map/all_to_all | solution.py:76
  249.5 2.9 %multiply_reduce_fusion.1 = (f32[256]{0:T(256)S(1)}, f32[256,384]{1,0:T(8,128)}) fusion(bf16[384,1536]{0,1:T(8,128)(2,1)S(1)} %bitcast.87, s32[1536]{0:T(1024)} %subtract_select_fusion, pred[1536]{0:T(1024)(128)(4,1)} %lt.182, f32[256,3072]{1,0:T(8,128)} %convert_element_type.34, s32[]{:T(128)S(6)} %select_n.231), kind=kOutput, calls=%fused_computation.25 | convolution fusion | flops 303070976 | bytes 1974788 | tf_op jit(solution)/shard_map/dot_general | solution.py:81
  252.4 0.6 broadcast_in_dim.111
  253.0 7.0 %all-to-all-start.2 = ((f32[8,1,256]{2,1,0:T(1,128)}), f32[8,1,256]{2,1,0:T(1,128)S(1)}, u32[]{:S(2)}, u32[]{:S(2)}) async-start(f32[8,1,256]{2,1,0:T(1,128)} %broadcast_in_dim.111), calls=%async_computation.2 | async-start | bytes 16384 | tf_op jit(solution)/shard_map/all_to_all | solution.py:11
  260.0 4.6 %all-to-all-done.2 = f32[8,1,256]{2,1,0:T(1,128)S(1)} async-done(((f32[8,1,256]{2,1,0:T(1,128)}), f32[8,1,256]{2,1,0:T(1,128)S(1)}, u32[]{:S(2)}, u32[]{:S(2)}) %all-to-all-start.2) | async-done | bytes 8224 | tf_op jit(solution)/shard_map/all_to_all | solution.py:11
  264.6 1.8 multiply_convert_fusion.2
  (22 shorter events, 0.1 us)
Async XLA Ops:
  6.5 129.0 %copy-start = (bf16[1,384,3072]{2,1,0:T(8,128)(2,1)S(1)}, bf16[1,384,3072]{2,1,0:T(8,128)(2,1)}, u32[]{:S(2)}) copy-start(bf16[1,384,3072]{2,1,0:T(8,128)(2,1)} %param.16) | copy-start | bytes 7077892
  6.5 2.0 copy-start.2
  8.6 2.1 copy-start.1
  10.8 0.7 copy-start.3
  12.3 13.7 %copy-start.5 = (s32[32,32]{1,0:T(8,128)}, s32[32,32]{1,0:T(8,128)S(1)}, u32[]{:S(2)}) copy-start(s32[32,32]{1,0:T(8,128)S(1)} %sub.52) | copy-start | bytes 12292
  12.7 0.6 copy-start.4
  36.1 40.5 %all-to-all-start = ((bf16[32,48,384]{2,1,0:T(8,128)(2,1)}), bf16[32,48,384]{2,1,0:T(8,128)(2,1)S(1)}, u32[]{:S(2)}, u32[]{:S(2)}) async-start(bf16[32,48,384]{2,1,0:T(8,128)(2,1)} %broadcast_select_fusion), calls=%async_computation | async-start | bytes 2359296 | tf_op jit(solution)/shard_map/all_to_all | solution.py:57
  48.0 79.5 %all-gather.2.cloned.1.call-start = ((), (), s32[]{:S(2)}) async-start(), calls=%async_computation.4 | async-start | bytes 7077888 | tf_op jit(solution)/shard_map/all_gather | solution.py:59
  83.9 116.1 %reduce-scatter.4.cloned.1.call-start = ((), (), s32[]{:S(2)}) async-start(), calls=%async_computation.5 | async-start | bytes 7077888
  155.6 46.7 %copy-start.6 = (f32[1,1024]{1,0:T(1,128)S(1)}, f32[1,1024]{1,0:T(1,128)}, u32[]{:S(2)}) copy-start(f32[1,1024]{1,0:T(1,128)} %param.13) | copy-start | bytes 12292
  211.5 38.0 %all-to-all-start.1 = ((bf16[384,32,48]{0,2,1:T(8,128)(2,1)}), bf16[384,32,48]{0,2,1:T(8,128)(2,1)S(1)}, u32[]{:S(2)}, u32[]{:S(2)}) async-start(bf16[384,32,48]{0,2,1:T(8,128)(2,1)} %broadcast_select_fusion.1), calls=%async_computation.1 | async-start | bytes 2359296 | tf_op jit(solution)/shard_map/all_to_all | solution.py:76
  225.8 34.2 %copy-start.7 = (bf16[384]{0:T(512)(128)(2,1)S(1)}, bf16[384]{0:T(512)(128)(2,1)}, u32[]{:S(2)}) copy-start(bf16[384]{0:T(512)(128)(2,1)} %param.17) | copy-start | bytes 2308
  253.0 11.6 %all-to-all-start.2 = ((f32[8,1,256]{2,1,0:T(1,128)}), f32[8,1,256]{2,1,0:T(1,128)S(1)}, u32[]{:S(2)}, u32[]{:S(2)}) async-start(f32[8,1,256]{2,1,0:T(1,128)} %broadcast_in_dim.111), calls=%async_computation.2 | async-start | bytes 16384 | tf_op jit(solution)/shard_map/all_to_all | solution.py:11
Sparse Core Ops, SparseCore 0:
  84.0 43.4 all-gather.1
  155.7 44.2 reduce-scatter.3
where the time goes:
time: 275 us; the launch traced here: 273 us
  waiting for transfers between devices  120 us (44%)
  local copies, waits for them, and re-layouts  47.3 us (17%)
  other arithmetic  41.2 us (15%)
  starting transfers between devices  28.5 us (10%)
  matrix products  22.3 us (8%)
  between operations  13.6 us (5%)
    all_gather x1, waiting for transfers between devices, on_device(): piece = lax.all_gather(shared, 'tp', axis=1, tiled=True)  43.6 us
    unnamed x3, waiting for transfers between devices  43.4 us
    all_to_all x1, waiting for transfers between devices, on_device(): lax.all_to_all(leaving, 'ep', split_axis=1, concat_axis=1, tiled=True)  23.7 us
    and x1, other arithmetic, on_device(): shared = jnp.take(arrived.reshape(-1, share_width), arrival, axis=0)  16.2 us
    gather x3, local copies, waits for them, and re-layouts, on_device(): jnp.take_along_axis(chosen, send_pos, axis=1) - device * tok_rows  12.8 us
    unnamed x18, local copies, waits for them, and re-layouts  12.3 us
    all_to_all x1, starting transfers between devices, on_device(): lax.all_to_all(outgoing, 'ep', split_axis=0, concat_axis=0, tiled=True)  11.9 us
    dot_general x1, matrix products, on_device(): lax.dot_general(piece, hidden, (((0,), (1,)), ((), ())), preferred_elemen...  11.4 us
  transfers between devices with their start and end apart: 5, of which 5 were waited for; matrix products, arithmetic and copies ran while one was open for 11% of the time, Pallas kernels for 0%

commit v1 on v0

v1 whole, which is shorter than its diff:
```python
import jax
import jax.numpy as jnp
from jax import lax
from jax.experimental import pallas as pl
from jax.experimental.pallas import tpu as pltpu
from jax.sharding import PartitionSpec as P

EPSILON = 1e-06
MESH = pl.DeviceIdType.MESH
F32, BF16 = jnp.float32, jnp.bfloat16

NZ, NX, NY = 8, 4, 4
EP, TP = NZ * NX, NY * 2
TOK, WIDTH, PICKS = 256, 3072, 1024
SHARE = WIDTH // TP
SLOTS = 48
ROWS = EP * SLOTS
LANE = 128
CHUNKS = SHARE // LANE
HALF = PICKS // 2
STEP = 256


def dot(a, b):
    return jnp.dot(a, b, preferred_element_type=F32)


def columns_of(row):
    return jnp.broadcast_to(row, (LANE, LANE)).T


def kernel(
    stream, gain_in, gain_out, local_row, arrival_row, affinity_row, gate_hbm, up_hbm, down_hbm,
    out,
    gate_w, up_w, down_w, scaled, place, place_t, pick, pick_t, weight_col,
    sending, arrived, picked, gate_acc, up_acc, hidden,
    own_acc, twin_out, twin_in, sums, ring_l, ring_r, fin_l, fin_r, weighted,
    leaving, returned, merged, totals,
    load_sem, out_send, out_recv, ag_send, ag_recv, rs_send, rs_recv, back_send, back_recv,
    tot_send, tot_recv,
):
    me = lax.axis_index("ep")
    tp = lax.axis_index("tp")
    z, x = me // NX, me % NX
    y, core = tp // 2, tp % 2
    y_r, y_l, y_f = (y + 1) % NY, (y + NY - 1) % NY, (y + 2) % NY
    right = (me, y_r * 2 + core)
    left = (me, y_l * 2 + core)
    twin = (me, y * 2 + 1 - core)

    def peer(j):
        jz, jx = j % NZ, j // NZ
        odd = jz % 2
        dz = odd * ((jz + 1) // 2) + (1 - odd) * ((NZ - jz // 2) % NZ)
        return ((z + dz) % NZ) * NX + (x + jx) % NX

    loads = [
        pltpu.make_async_copy(src, dst, load_sem.at[i])
        for i, (src, dst) in enumerate(((gate_hbm, gate_w), (up_hbm, up_w), (down_hbm, down_w)))
    ]
    for load in loads:
        load.start()

    barrier = pltpu.get_barrier_semaphore()

    @pl.loop(1, EP)
    def _(j):
        pl.semaphore_signal(barrier, inc=1, device_id=(peer(j), tp), device_id_type=MESH)

    @pl.loop(1, TP)
    def _(j):
        pl.semaphore_signal(barrier, inc=1, device_id=(me, (tp + j) % TP), device_id_type=MESH)

    own_lanes = pl.ds(pl.multiple_of(tp * SHARE, LANE), SHARE)

    @pl.loop(0, TOK // 32)
    def _(i):
        rows = pl.ds(pl.multiple_of(i * 32, 32), 32)
        wide = stream[rows, :].astype(F32)
        scale = lax.rsqrt(jnp.sum(wide * wide, axis=1, keepdims=True) / WIDTH + EPSILON)
        own = stream[rows, own_lanes].astype(F32)
        scaled[rows, :] = (own * scale * gain_in[:, own_lanes].astype(F32)).astype(BF16)

    @pl.loop(0, ROWS // LANE)
    def _(i):
        rows = pl.ds(pl.multiple_of(i * LANE, LANE), LANE)
        column = columns_of(local_row[:, rows])
        for b in range(TOK // LANE):
            lanes = lax.broadcasted_iota(jnp.int32, (LANE, LANE), 1) + b * LANE
            place[rows, b * LANE:(b + 1) * LANE] = jnp.where(column == lanes, 1.0, 0.0).astype(BF16)

    @pl.loop(0, EP // 8)
    def _(i):
        rows = pl.ds(pl.multiple_of(i * 8 * SLOTS, LANE), 8 * SLOTS)
        taken = dot(place[rows, :], scaled[...]).astype(BF16)
        for k in range(CHUNKS):
            sending[k, pl.ds(i * 8, 8)] = taken[:, k * LANE:(k + 1) * LANE].reshape(8, SLOTS, LANE)

    pl.semaphore_wait(barrier, EP - 1 + TP - 1)

    def exchange(source, target, send, recv, k):
        @pl.loop(1, EP)
        def _(j):
            other = peer(j)
            pltpu.make_async_remote_copy(
                src_ref=source.at[k, other], dst_ref=target.at[k, me],
                send_sem=send.at[k], recv_sem=recv.at[k],
                device_id=(other, tp), device_id_type=MESH,
            ).start()

    def exchange_wait(target, sem, k):
        whole = target.at[k, pl.ds(0, EP - 1)]
        pltpu.make_async_copy(whole, whole, sem.at[k]).wait()

    for k in range(CHUNKS):
        exchange(sending, arrived, out_send, out_recv, k)
    for k in range(CHUNKS):
        arrived[k, me] = sending[k, me]

    @pl.loop(0, PICKS // LANE)
    def _(i):
        rows = pl.ds(pl.multiple_of(i * LANE, LANE), LANE)
        column = columns_of(arrival_row[:, rows])
        for b in range(ROWS // LANE):
            lanes = lax.broadcasted_iota(jnp.int32, (LANE, LANE), 1) + b * LANE
            pick[rows, b * LANE:(b + 1) * LANE] = jnp.where(column == lanes, 1.0, 0.0).astype(BF16)
        weight_col[rows, :] = columns_of(affinity_row[:, rows])

    @pl.loop(0, ROWS // LANE)
    def _(i):
        rows = pl.ds(pl.multiple_of(i * LANE, LANE), LANE)
        subl = lax.broadcasted_iota(jnp.int32, (LANE, PICKS), 0) + i * LANE
        pick_t[rows, :] = jnp.where(arrival_row[...] == subl, 1.0, 0.0).astype(BF16)

    for b in range(TOK // LANE):
        rows = slice(b * LANE, (b + 1) * LANE)
        subl = lax.broadcasted_iota(jnp.int32, (LANE, ROWS), 0) + b * LANE
        place_t[rows, :] = jnp.where(local_row[...] == subl, 1.0, 0.0).astype(BF16)

    top, bottom = pl.ds(0, HALF), pl.ds(HALF, HALF)

    def ag(k, i, block, rows, to):
        ref = picked.at[k, block] if rows is None else picked.at[k, block, rows]
        return pltpu.make_async_remote_copy(
            src_ref=ref, dst_ref=ref, send_sem=ag_send.at[k, i], recv_sem=ag_recv.at[k, i],
            device_id=to, device_id_type=MESH,
        )

    b_r, b_l, b_f = y_r * 2 + core, y_l * 2 + core, y_f * 2 + core
    t_r, t_l, t_f, t_o = (y_r * 2 + 1 - core, y_l * 2 + 1 - core, y_f * 2 + 1 - core, y * 2 + 1 - core)
    ag_plan = (
        (tp, top, right), (tp, bottom, right), (b_l, top, right),
        (tp, bottom, left), (tp, top, left), (b_r, bottom, left),
        (tp, None, twin),
        (b_l, top, twin), (b_l, bottom, twin), (b_f, top, twin),
        (b_r, bottom, twin), (b_r, top, twin), (b_f, bottom, twin),
    )
    ag_lands = (
        (b_l, top), (b_l, bottom), (b_f, top),
        (b_r, bottom), (b_r, top), (b_f, bottom),
        (t_o, None),
        (t_l, top), (t_l, bottom), (t_f, top),
        (t_r, bottom), (t_r, top), (t_f, bottom),
    )

    def ag_start(k, i):
        block, rows, to = ag_plan[i]
        ag(k, i, block, rows, to).start()

    def ag_arrive(k, i):
        block, rows = ag_lands[i]
        ag(k, i, block, rows, twin).wait_recv()

    def compact(k):
        exchange_wait(arrived, out_recv, k)

        @pl.loop(0, PICKS // STEP)
        def _(i):
            rows = pl.ds(pl.multiple_of(i * STEP, STEP), STEP)
            picked[k, tp, rows, :] = dot(pick[rows, :], arrived[k].reshape(ROWS, LANE)).astype(BF16)

        for i in (0, 3, 1, 4, 6):
            ag_start(k, i)

    def ag_forward(k):
        ag_arrive(k, 0)
        ag_start(k, 2)
        ag_arrive(k, 3)
        ag_start(k, 5)
        ag_start(k, 7)
        ag_start(k, 10)

    def ag_rest(k):
        for i in (1, 4, 2, 5):
            ag_arrive(k, i)
            ag_start(k, i + 7 if i in (1, 2) else i + 7)

    def project(k):
        for i in range(6, 13):
            ag_arrive(k, i)

        @pl.loop(0, PICKS // STEP)
        def _(i):
            rows = pl.ds(pl.multiple_of(i * STEP, STEP), STEP)
            lhs = jnp.concatenate([picked[k, b, rows, :] for b in range(TP)], axis=1)
            for weights, acc in ((gate_w, gate_acc), (up_w, up_acc)):
                rhs = jnp.concatenate(
                    [weights[pl.ds(b * SHARE + k * LANE, LANE), :] for b in range(TP)], axis=0
                )
                part = dot(lhs, rhs)
                if k == 0:
                    acc[rows, :] = part
                elif k < CHUNKS - 1:
                    acc[rows, :] += part
                else:
                    total = acc[rows, :] + part
                    if acc is gate_acc:
                        gate = total
                    else:
                        hidden[rows, :] = (gate / (1.0 + jnp.exp(-gate)) * total).astype(BF16)

    compact(0)
    ag_forward(0)
    compact(1)
    ag_rest(0)
    loads[0].wait()
    loads[1].wait()
    project(0)
    ag_forward(1)
    compact(2)
    ag_rest(1)
    project(1)
    ag_forward(2)
    ag_rest(2)
    project(2)
    loads[2].wait()

    def rs(k, i, src, dst, to):
        return pltpu.make_async_remote_copy(
            src_ref=src, dst_ref=dst, send_sem=rs_send.at[k, i], recv_sem=rs_recv.at[k, i],
            device_id=to, device_id_type=MESH,
        )

    def rs_copy(k, i):
        return (
            lambda: rs(k, 0, twin_out.at[k], twin_in.at[k], twin),
            lambda: rs(k, 1, sums.at[k, y_f, top], ring_l.at[k], right),
            lambda: rs(k, 2, sums.at[k, y_f, bottom], ring_r.at[k], left),
            lambda: rs(k, 3, sums.at[k, y_r, bottom], fin_l.at[k, bottom], right),
            lambda: rs(k, 4, sums.at[k, y_l, top], fin_r.at[k, top], left),
            lambda: rs(k, 5, sums.at[k, y_r, top], fin_l.at[k, top], right),
            lambda: rs(k, 6, sums.at[k, y_l, bottom], fin_r.at[k, bottom], left),
        )[i]()

    def down(k):
        def part(which, target):
            @pl.loop(0, PICKS // STEP)
            def _(i):
                rows = pl.ds(pl.multiple_of(i * STEP, STEP), STEP)
                lhs = hidden[rows, :]
                for pair in range(NY // 2):
                    pieces = []
                    for q in (2 * pair, 2 * pair + 1):
                        start = pl.multiple_of((2 * q + which) * SHARE + k * LANE, LANE)
                        pieces.append(down_w[:, pl.ds(start, LANE)])
                    res = dot(lhs, jnp.concatenate(pieces, axis=1))
                    for n, q in enumerate((2 * pair, 2 * pair + 1)):
                        piece = res[:, n * LANE:(n + 1) * LANE]
                        if target is own_acc:
                            own_acc[q, rows, :] = piece
                        else:
                            target[k, q, rows, :] = piece.astype(BF16)

        part(1 - core, twin_out)
        rs_copy(k, 0).start()
        part(core, own_acc)
        rs_copy(k, 0).wait_recv()

        @pl.loop(0, NY * PICKS // STEP)
        def _(i):
            q = i // (PICKS // STEP)
            rows = pl.ds(pl.multiple_of((i % (PICKS // STEP)) * STEP, STEP), STEP)
            sums[k, q, rows, :] = (own_acc[q, rows, :] + twin_in[k, q, rows, :].astype(F32)).astype(BF16)

        for i in (1, 2, 3, 4):
            rs_copy(k, i).start()

    def rs_forward(k):
        for i, ring, q, rows in ((1, ring_l, y_r, top), (2, ring_r, y_l, bottom)):
            rs_copy(k, i).wait_recv()
            sums[k, q, rows, :] = (
                sums[k, q, rows, :].astype(F32) + ring[k].astype(F32)
            ).astype(BF16)
            rs_copy(k, i + 4).start()

    def give_back(k):
        for i in (3, 4, 5, 6):
            rs_copy(k, i).wait_recv()

        @pl.loop(0, PICKS // STEP)
        def _(i):
            rows = pl.ds(pl.multiple_of(i * STEP, STEP), STEP)
            total = (
                sums[k, y, rows, :].astype(F32) + fin_l[k, rows, :].astype(F32)
                + fin_r[k, rows, :].astype(F32)
            )
            weighted[rows, :] = (total * weight_col[rows, :]).astype(BF16)

        @pl.loop(0, EP // 8)
        def _(i):
            rows = pl.ds(pl.multiple_of(i * 8 * SLOTS, LANE), 8 * SLOTS)
            slab = dot(pick_t[rows, :], weighted[...]).astype(BF16)
            leaving[k, pl.ds(i * 8, 8)] = slab.reshape(8, SLOTS, LANE)

        exchange(leaving, returned, back_send, back_recv, k)
        returned[k, me] = leaving[k, me]

    down(0)
    rs_forward(0)
    down(1)
    give_back(0)
    rs_forward(1)
    down(2)
    give_back(1)
    rs_forward(2)
    give_back(2)

    square = jnp.zeros((TOK, LANE), F32)
    for k in range(CHUNKS):
        exchange_wait(returned, back_recv, k)
        lanes = pl.ds(pl.multiple_of(tp * SHARE + k * LANE, LANE), LANE)
        part = stream[:, lanes].astype(F32) + dot(place_t[...], returned[k].reshape(ROWS, LANE))
        merged[k] = part
        square = square + part * part
    totals[tp] = jnp.broadcast_to(jnp.sum(square.T, axis=0, keepdims=True), (8, TOK))

    def total_copy(j, block):
        return pltpu.make_async_remote_copy(
            src_ref=totals.at[block], dst_ref=totals.at[block],
            send_sem=tot_send.at[j], recv_sem=tot_recv.at[j],
            device_id=(me, (tp + j) % TP), device_id_type=MESH,
        )

    for j in range(1, TP):
        total_copy(j, tp).start()
    for j in range(1, TP):
        total_copy(j, (tp + TP - j) % TP).wait_recv()
    whole = totals[0]
    for b in range(1, TP):
        whole = whole + totals[b]
    for b in range(TOK // LANE):
        rows = slice(b * LANE, (b + 1) * LANE)
        scale = lax.rsqrt(columns_of(whole[0:1, rows]) / WIDTH + EPSILON)
        for k in range(CHUNKS):
            lanes = slice(k * LANE, (k + 1) * LANE)
            out[rows, lanes] = (merged[k, rows, :] * scale * gain_out[:, lanes].astype(F32)).astype(BF16)

    for k in range(CHUNKS):
        exchange_wait(sending, out_send, k)
        exchange_wait(leaving, back_send, k)
        for i in range(13):
            block, rows, to = ag_plan[i]
            ag(k, i, block, rows, to).wait_send()
        for i in range(7):
            rs_copy(k, i).wait_send()
    for j in range(1, TP):
        total_copy(j, tp).wait_send()


def whole_layer(stream, gain_in, gain_out, local_row, arrival_row, affinity_row, gate, up, down):
    vmem = pl.BlockSpec(memory_space=pltpu.VMEM)
    hbm = pl.BlockSpec(memory_space=pl.ANY)
    dma = pltpu.SemaphoreType.DMA
    return pl.pallas_call(
        kernel,
        out_shape=jax.ShapeDtypeStruct((TOK, SHARE), BF16),
        in_specs=[vmem] * 6 + [hbm] * 3,
        out_specs=vmem,
        scratch_shapes=[
            pltpu.VMEM((WIDTH, SHARE), BF16),
            pltpu.VMEM((WIDTH, SHARE), BF16),
            pltpu.VMEM((SHARE, WIDTH), BF16),
            pltpu.VMEM((TOK, SHARE), BF16),
            pltpu.VMEM((ROWS, TOK), BF16),
            pltpu.VMEM((TOK, ROWS), BF16),
            pltpu.VMEM((PICKS, ROWS), BF16),
            pltpu.VMEM((ROWS, PICKS), BF16),
            pltpu.VMEM((PICKS, LANE), F32),
            pltpu.VMEM((CHUNKS, EP, SLOTS, LANE), BF16),
            pltpu.VMEM((CHUNKS, EP, SLOTS, LANE), BF16),
            pltpu.VMEM((CHUNKS, TP, PICKS, LANE), BF16),
            pltpu.VMEM((PICKS, SHARE), F32),
            pltpu.VMEM((PICKS, SHARE), F32),
            pltpu.VMEM((PICKS, SHARE), BF16),
            pltpu.VMEM((NY, PICKS, LANE), F32),
            pltpu.VMEM((CHUNKS, NY, PICKS, LANE), BF16),
            pltpu.VMEM((CHUNKS, NY, PICKS, LANE), BF16),
            pltpu.VMEM((CHUNKS, NY, PICKS, LANE), BF16),
            pltpu.VMEM((CHUNKS, HALF, LANE), BF16),
            pltpu.VMEM((CHUNKS, HALF, LANE), BF16),
            pltpu.VMEM((CHUNKS, PICKS, LANE), BF16),
            pltpu.VMEM((CHUNKS, PICKS, LANE), BF16),
            pltpu.VMEM((PICKS, LANE), BF16),
            pltpu.VMEM((CHUNKS, EP, SLOTS, LANE), BF16),
            pltpu.VMEM((CHUNKS, EP, SLOTS, LANE), BF16),
            pltpu.VMEM((CHUNKS, TOK, LANE), F32),
            pltpu.VMEM((TP, 8, TOK), F32),
            dma((3,)),
            dma((CHUNKS,)),
            dma((CHUNKS,)),
            dma((CHUNKS, 13)),
            dma((CHUNKS, 13)),
            dma((CHUNKS, 7)),
            dma((CHUNKS, 7)),
            dma((CHUNKS,)),
            dma((CHUNKS,)),
            dma((TP,)),
            dma((TP,)),
        ],
        compiler_params=pltpu.CompilerParams(
            collective_id=0, has_side_effects=True, vmem_limit_bytes=60 * 1024 * 1024
        ),
        name="whole_layer",
    )(stream, gain_in, gain_out, local_row, arrival_row, affinity_row, gate, up, down)


def on_device(stream, ffn_gain, chosen, affinity, w_gate, w_up, w_down, final_gain):
    me = lax.axis_index("ep")
    first = jnp.sum((chosen < me * TOK).astype(jnp.int32), axis=1)
    last = jnp.sum((chosen < (me + 1) * TOK).astype(jnp.int32), axis=1)
    slot = jnp.arange(SLOTS, dtype=jnp.int32)
    position = first[:, None] + slot[None, :]
    hit = position[:, :, None] == jnp.arange(PICKS, dtype=jnp.int32)[None, None, :]
    token = jnp.sum(jnp.where(hit, chosen[:, None, :], 0), axis=2) - me * TOK
    local = jnp.where(position < last[:, None], token, -1)
    own = lax.dynamic_index_in_dim(chosen, me, 0, keepdims=False)
    source = own // TOK
    starts = jnp.sum((source[None, :] < jnp.arange(EP, dtype=jnp.int32)[:, None]).astype(jnp.int32), axis=1)
    start = jnp.sum(
        jnp.where(source[None, :] == jnp.arange(EP, dtype=jnp.int32)[:, None], starts[:, None], 0), axis=0
    )
    arrival = source * SLOTS + jnp.arange(PICKS, dtype=jnp.int32) - start
    return whole_layer(
        stream, ffn_gain.reshape(1, -1), final_gain.reshape(1, -1), local.reshape(1, -1),
        arrival.reshape(1, -1), affinity, w_gate[0], w_up[0], w_down[0],
    )


def solution(mesh):
    return jax.shard_map(
        on_device,
        mesh=mesh,
        in_specs=(
            P("ep", None),
            P(),
            P(),
            P("ep", None),
            P("ep", None, "tp"),
            P("ep", None, "tp"),
            P("ep", "tp", None),
            P("tp"),
        ),
        out_specs=P("ep", "tp"),
        check_vma=False,
    )
```

time: 275 us -> 126 us (0.46)
  waiting for transfers between devices: 120 us -> 0 us
  Pallas kernels: 0 us -> 115 us
  local copies, waits for them, and re-layouts: 47.3 us -> 4.85 us
  other arithmetic: 41.2 us -> 5.71 us
  starting transfers between devices: 28.5 us -> 0 us
  matrix products: 22.3 us -> 0 us
  between operations: 13.6 us -> 0.03 us
    pallas_call x0 -> x1, Pallas kernels: none -> 115 us  [whole_layer(): pl.pallas_call(kernel, out_shape=jax.ShapeDtypeStruct((TOK, SHARE), BF16)...]
    all_gather x1 -> x0, waiting for transfers between devices: 43.6 us -> none  [on_device(): piece = lax.all_gather(shared, 'tp', axis=1, tiled=True)]
    unnamed x3 -> x0, waiting for transfers between devices: 43.4 us -> none
    all_to_all x3 -> x0, waiting for transfers between devices: 33.4 us -> none  [the longest x1 23.7 us: on_device(): lax.all_to_all(leaving, 'ep', split_axis=1, concat_axis=1, tiled=True)]
    gather x8 -> x0, local copies, waits for them, and re-layouts: 29.8 us -> none  [the longest x3 12.8 us: on_device(): jnp.take_along_axis(chosen, send_pos, axis=1) - device * tok_rows]
    all_to_all x3 -> x0, starting transfers between devices: 28.4 us -> none  [the longest x1 11.9 us: on_device(): lax.all_to_all(outgoing, 'ep', split_axis=0, concat_axis=0, tiled=True)]
    dot_general x3 -> x0, matrix products: 22.3 us -> none  [the longest x1 11.4 us: on_device(): lax.dot_general(piece, hidden, (((0,), (1,)), ((), ())), preferred_elemen...]
    and x3 -> x0, other arithmetic: 16.4 us -> none  [the longest x1 16.2 us: on_device(): shared = jnp.take(arrived.reshape(-1, share_width), arrival, axis=0)]
  transfers between devices with their start and end apart: 5 -> 0, of which waited for: 5 -> 0; matrix products, arithmetic and copies ran while one was open for 11% -> 0% of each run, Pallas kernels for 0% -> 0%
where the time goes in v1:
time: 126 us
  Pallas kernels  115 us (91%)
  other arithmetic  5.71 us (5%)
  local copies, waits for them, and re-layouts  4.85 us (4%)
    pallas_call x1, Pallas kernels, whole_layer(): pl.pallas_call(kernel, out_shape=jax.ShapeDtypeStruct((TOK, SHARE), BF16)...  115 us

profile of v1, /device:TPU:1, one launch (start us, length us, event | category | flops | bytes accessed | tf_op | source)
XLA Modules:
  0.0 125.8 jit_solution(2149850059432410520)
XLA Ops:
  0.0 1.0 convert_reduce_fusion.1
  1.0 1.2 reshape.86.gain_out
  2.3 0.8 and_select_fusion
  3.1 0.1 convert_reduce_fusion
  3.2 0.1 select_reduce_fusion.1
  3.3 1.4 %add_subtract_fusion.arrival_row = s32[1,1024]{1,0:T(1,128)} fusion(s32[1,1024]{1,0:T(1,128)S(1)} %bitcast.10, s32[32,1024]{1,0:T(8,128)} %param.10, s32[]{:T(128)S(6)} %select_n.36), kind=kLoop, calls=%fused_computation.14 | loop fusion | flops 18432 | bytes 12292 | tf_op jit(solution)/shard_map/sub | solution.py:442
  4.7 1.3 %reshape.85.gain_in = bf16[1,3072]{1,0:T(2,128)(2,1)} reshape(bf16[3072]{0:T(1024)(128)(2,1)} %param.9) | data formatting | bytes 12288 | tf_op jit(solution)/shard_map/reshape | solution.py:444
  6.0 0.1 iota_add_fusion
  6.0 2.1 %select_reduce_fusion = s32[32,48]{1,0:T(8,128)S(1)} fusion(s32[32,1024]{1,0:T(8,128)} %param.10, s32[32,48]{1,0:T(8,128)S(1)} %iota_add_fusion), kind=kLoop, calls=%fused_computation | loop fusion | flops 4717056 | bytes 143360 | tf_op jit(solution)/shard_map/reduce_sum | solution.py:434
  8.2 0.1 subtract_select_fusion
  8.3 0.7 select_n.35.local_row
  8.9 115.2 %whole_layer.1 = bf16[256,384]{1,0:T(8,128)(2,1)} custom-call(bf16[256,3072]{1,0:T(8,128)(2,1)} %stream.1, bf16[1,3072]{1,0:T(2,128)(2,1)} %reshape.85.gain_in, bf16[1,384]{1,0:T(2,128)(2,1)} %reshape.86.gain_out, s32[1,1536]{1,0:T(1,128)} %select_n.35.local_row, s32[1,1024]{1,0:T(1,128)} %add_subtract_fusion.arrival_row, f32[1,1024]{1,0:T(1,128)} %affinity_row.1, ...), custom_call_target="tpu_custom_call" | custom-call | tf_op jit(solution)/shard_map/whole_layer/pallas_call | solution.py:374
  124.1 1.6 %copy.10 = bf16[256,384]{1,0:T(8,128)(2,1)} copy(bf16[256,384]{1,0:T(8,128)(2,1)} %whole_layer.1) | data formatting | bytes 393216
